TPU v7x, 32 devices: a whole 2x2x4 slice. The times are simulated.
32 devices in a mesh: ep: 8 (over z, core), tp: 4 (over y, x).
Axes of the slice: x: 2, y: 2, z: 4, core: 2. Of those that a mesh axis runs over, the one named last changes fastest.
Arguments:
- resid: bfloat16 [32, 2048], P('ep', 'tp'), may hold values from -6 to 6
- cache_key: bfloat16 [32, 8, 224, 256], P(('ep', 'tp')), may hold values from -360 to 360
- cache_value: bfloat16 [32, 8, 224, 256], P(('ep', 'tp')), may hold values from -6 to 6
- lengths: int32 [32], P(('ep', 'tp')), may hold values from 28 to 224
- lambdas: float32 [8], replicated, may hold values from 0.3 to 0.8
- mix_gain: float32 [2048], replicated, may hold values from 0.1 to 1.9
- query_gain: float32 [128], replicated, may hold values from 0.1 to 1.9
- key_gain: float32 [128], replicated, may hold values from 0.1 to 1.9
- sub_gain: float32 [256], replicated, may hold values from 0.1 to 1.9
- ffn_gain: float32 [2048], replicated, may hold values from 0.1 to 1.9
- w_query: bfloat16 [2048, 2048], P(None, 'tp'), may hold values from -0.125 to 0.125
- w_key: bfloat16 [2048, 2048], P(None, 'tp'), may hold values from -0.125 to 0.125
- w_value: bfloat16 [2048, 2048], P(None, 'tp'), may hold values from -0.125 to 0.125
- w_out: bfloat16 [2048, 2048], P(None, 'tp'), may hold values from -0.125 to 0.125
- routes: int32 [32, 2], P('ep'), may hold values from 0 to 7, all different within a row; in each aligned block of 4 rows (0 to 3, 4 to 7, ...) at most 4 rows name the same one
- route_weights: float32 [32, 2], P('ep'), may hold values from 0.2 to 0.8
- w_gate: bfloat16 [8, 2048, 4096], P('ep', None, 'tp'), may hold values from -0.125 to 0.125
- w_up: bfloat16 [8, 2048, 4096], P('ep', None, 'tp'), may hold values from -0.125 to 0.125
- w_down: bfloat16 [8, 4096, 2048], P('ep', 'tp'), may hold values from -0.09375 to 0.09375
Outputs:
- result: bfloat16 [32, 2048], P('ep', 'tp')
- new_key: bfloat16 [32, 8, 256], P(('ep', 'tp'))
- new_value: bfloat16 [32, 8, 256], P(('ep', 'tp'))
Inputs may be any that keep to these rules, and one draw needn't show every extreme that they name: `routes`: within the 4 rows of one index of ep no expert is named more than 4 times, and in some of them one expert is named exactly 4 times; the two experts of a row differ. `lengths`: every sequence has at least two live positions.
All inputs are finite; a program needn't handle non-finite values.
Results may differ from a plain program's by a relative error of at most 0.0099.
Values may be sent and summed in bfloat16 or wider, within the bound.
A program may use at most 64 MiB of HBM per device.

v0:
```python
import math
import jax
import jax.numpy as jnp
from jax import lax
from jax.sharding import PartitionSpec as P

CAP = 4
epsilon = 1e-06
out_factor = 0.2 + 0.6 * math.exp(-0.3)
masked_score = -1e30


def scaled_rows(values, gain):
    wide = values.astype(jnp.float32)
    return wide * lax.rsqrt(jnp.mean(wide * wide, axis=-1, keepdims=True) + epsilon) * gain


def route_tables(routes, route_weights, experts, capacity):
    flat_routes = routes.reshape(-1)
    expert_hit = (flat_routes[:, None] == jnp.arange(experts, dtype=jnp.int32)[None, :]).astype(
        jnp.int32
    )
    before = jnp.cumsum(expert_hit, axis=0) - expert_hit
    slot_index = jnp.sum(before * expert_hit, axis=1)
    slot_hit = (slot_index[:, None] == jnp.arange(capacity, dtype=jnp.int32)[None, :]).astype(
        jnp.float32
    )
    pair_table = expert_hit.astype(jnp.float32)[:, :, None] * slot_hit[:, None, :]
    pair_table = pair_table.reshape(routes.shape[0], 2, experts, capacity)
    dispatch = jnp.sum(pair_table, axis=1)
    combine = jnp.sum(pair_table * route_weights[:, :, None, None], axis=1)
    return (dispatch, combine)


def attend(
    queries,
    key_rows,
    value_rows,
    past_keys,
    past_values,
    live_len,
    lambdas,
    query_gain,
    key_gain,
    sub_gain,
):
    seq_count, kv_heads, cache_len, key_width = past_keys.shape
    head_dim = key_width // 2
    head_count = lambdas.shape[0]
    group_size = head_count // kv_heads
    value_dim = past_values.shape[-1]
    score_scale = head_dim ** (-0.5)
    q_unit = scaled_rows(
        queries.reshape(seq_count, kv_heads, group_size, 2, head_dim), query_gain
    ).astype(jnp.bfloat16)
    new_key = scaled_rows(key_rows.reshape(seq_count, kv_heads, 2, head_dim), key_gain).astype(
        jnp.bfloat16
    )
    new_value = value_rows.reshape(seq_count, kv_heads, value_dim)
    past_split = past_keys.reshape(seq_count, kv_heads, cache_len, 2, head_dim)
    scores = (
        jnp.einsum("sjgmd,sjlmd->sjgml", q_unit, past_split, preferred_element_type=jnp.float32)
        * score_scale
    )
    own_score = (
        jnp.einsum("sjgmd,sjmd->sjgm", q_unit, new_key, preferred_element_type=jnp.float32)
        * score_scale
    )
    live_mask = jnp.arange(cache_len, dtype=jnp.int32)[None, :] < live_len[:, None]
    scores = jnp.where(live_mask[:, None, None, None, :], scores, masked_score)
    peak = jnp.maximum(jnp.max(scores, axis=-1), own_score)
    past_weight = jnp.exp(scores - peak[..., None])
    own_weight = jnp.exp(own_score - peak)
    totals = jnp.sum(past_weight, axis=-1) + own_weight
    past_prob = past_weight / totals[..., None]
    own_prob = own_weight / totals
    mix_lambda = lambdas.reshape(1, kv_heads, group_size, 1)
    past_mix = (past_prob[..., 0, :] - mix_lambda * past_prob[..., 1, :]).astype(jnp.bfloat16)
    own_mix = (own_prob[..., 0] - mix_lambda[..., 0] * own_prob[..., 1]).astype(jnp.bfloat16)
    head_out = jnp.einsum(
        "sjgl,sjlv->sjgv", past_mix, past_values, preferred_element_type=jnp.float32
    )
    head_out = (
        head_out
        + own_mix.astype(jnp.float32)[..., None] * new_value.astype(jnp.float32)[:, :, None, :]
    )
    mixed = (
        (scaled_rows(head_out, sub_gain) * out_factor)
        .astype(jnp.bfloat16)
        .reshape(seq_count, head_count * value_dim)
    )
    return (mixed, new_key.reshape(seq_count, kv_heads, key_width), new_value)


def local(
    resid,
    cache_key,
    cache_value,
    lengths,
    lambdas,
    mix_gain,
    query_gain,
    key_gain,
    sub_gain,
    ffn_gain,
    w_query,
    w_key,
    w_value,
    w_out,
    routes,
    route_weights,
    w_gate,
    w_up,
    w_down,
):
    gathered = lax.all_gather(resid, "tp", axis=1, tiled=True)
    normed = scaled_rows(gathered, mix_gain).astype(jnp.bfloat16)
    query_part = jnp.dot(normed, w_query, preferred_element_type=jnp.float32).astype(jnp.bfloat16)
    key_part = jnp.dot(normed, w_key, preferred_element_type=jnp.float32).astype(jnp.bfloat16)
    value_part = jnp.dot(normed, w_value, preferred_element_type=jnp.float32).astype(jnp.bfloat16)
    queries, key_rows, value_rows = (
        lax.all_to_all(query_part, "tp", split_axis=0, concat_axis=1, tiled=True),
        lax.all_to_all(key_part, "tp", split_axis=0, concat_axis=1, tiled=True),
        lax.all_to_all(value_part, "tp", split_axis=0, concat_axis=1, tiled=True),
    )
    mixed, new_key, new_value = attend(
        queries,
        key_rows,
        value_rows,
        cache_key,
        cache_value,
        lengths,
        lambdas,
        query_gain,
        key_gain,
        sub_gain,
    )
    attn_proj = jnp.dot(
        lax.all_gather(mixed, "tp", axis=0, tiled=True), w_out, preferred_element_type=jnp.float32
    )
    updated = (resid.astype(jnp.float32) + attn_proj).astype(jnp.bfloat16)
    updated_rows = lax.all_gather(updated, "tp", axis=1, tiled=True)
    hidden = scaled_rows(updated_rows, ffn_gain).astype(jnp.bfloat16)
    experts = w_gate.shape[0] * lax.axis_size("ep")
    dispatch, combine = route_tables(routes, route_weights, experts, CAP)
    send = jnp.einsum(
        "gec,gd->ecd", dispatch.astype(jnp.bfloat16), hidden, preferred_element_type=jnp.float32
    ).astype(jnp.bfloat16)
    slots = lax.all_to_all(send, "ep", split_axis=0, concat_axis=0, tiled=True)
    flat_rows = slots.reshape(-1, slots.shape[-1])
    gate_out = jnp.dot(flat_rows, w_gate[0], preferred_element_type=jnp.float32)
    up_out = jnp.dot(flat_rows, w_up[0], preferred_element_type=jnp.float32)
    act = (jax.nn.silu(gate_out) * up_out).astype(jnp.bfloat16)
    down_out = jnp.dot(act, w_down[0], preferred_element_type=jnp.float32)
    partial_value = down_out.reshape(slots.shape[0], slots.shape[1], down_out.shape[-1])
    flat_combine = combine.reshape(combine.shape[0], -1)
    summed = lax.psum_scatter(
        partial_value.astype(jnp.bfloat16), "tp", scatter_dimension=2, tiled=True
    ).astype(jnp.float32)
    returned = lax.all_to_all(
        summed.astype(jnp.bfloat16), "ep", split_axis=0, concat_axis=0, tiled=True
    ).astype(summed.dtype)
    expert_mix = jnp.dot(
        flat_combine,
        returned.reshape(-1, returned.shape[-1]),
        precision=lax.Precision.HIGHEST,
        preferred_element_type=jnp.float32,
    )
    result = (updated.astype(jnp.float32) + expert_mix).astype(jnp.bfloat16)
    return (result, new_key, new_value)


def solution(mesh):
    in_specs = (
        P("ep", "tp"),
        P(("ep", "tp"), None, None, None),
        P(("ep", "tp"), None, None, None),
        P(("ep", "tp")),
        P(),
        P(),
        P(),
        P(),
        P(),
        P(),
        P(None, "tp"),
        P(None, "tp"),
        P(None, "tp"),
        P(None, "tp"),
        P("ep", None),
        P("ep", None),
        P("ep", None, "tp"),
        P("ep", None, "tp"),
        P("ep", "tp", None),
    )
    out_specs = (P("ep", "tp"), P(("ep", "tp"), None, None), P(("ep", "tp"), None, None))
    return jax.shard_map(local, mesh=mesh, in_specs=in_specs, out_specs=out_specs, check_vma=False)
```

profile of v0, /device:TPU:0, one launch (start us, length us, event | category | flops | bytes accessed | tf_op | source)
XLA Modules:
  0.0 129.9 jit_solution(2296652605895860037)
XLA Ops:
  7.2 0.0 copy-start
  7.2 0.0 copy-start.3
  7.2 9.9 %all_gather.9 = bf16[4,2048]{1,0:T(4,128)(2,1)S(1)} all-gather(bf16[4,512]{1,0:T(4,128)(2,1)} %param.19), channel_id=1, replica_groups=mesh['ep'=8,'tp'=4] {'tp'}, dimensions={1}, use_global_device_ids=true | all-gather | bytes 20480 | tf_op jit(solution)/shard_map/all_gather | solution.py:116
  17.1 0.1 fusion.26
  17.3 1.1 fusion.18
  18.4 0.5 broadcast.214
  18.9 0.7 reduce.19
  19.6 0.6 reshape.382
  20.2 3.2 %all-to-all-start = ((bf16[4,2,256]{2,1,0:T(2,128)(2,1)}), bf16[4,2,256]{2,1,0:T(2,128)(2,1)S(1)}, u32[]{:S(2)}, u32[]{:S(2)}) async-start(bf16[4,2,256]{2,1,0:T(2,128)(2,1)} %reshape.382), calls=%async_computation | async-start | bytes 8192 | tf_op jit(solution)/shard_map/all_to_all | solution.py:122
  23.4 0.1 copy.64
  23.5 0.1 eq.47
  23.6 0.1 fusion.48
  23.7 2.1 %fusion.19 = bf16[4,1,512]{2,0,1:T(4,128)(2,1)S(1)} fusion(bf16[2048,512]{1,0:T(8,128)(2,1)} %param.30, bf16[4,2048]{1,0:T(4,128)(2,1)S(1)} %all_gather.9, f32[2048]{0:T(1024)S(1)} %copy-done.3, f32[4]{0:T(128)S(1)} %add_rsqrt_fusion.4), kind=kOutput, calls=%fused_computation.19 | convolution fusion | flops 8423424 | bytes 2125840 | tf_op jit(solution)/shard_map/dot_general | solution.py:119
  26.5 0.0 copy-start.10
  26.5 0.4 fusion.20
  27.0 0.1 fusion.51
  27.1 0.2 select_reduce_fusion
  27.2 0.1 eq.51
  27.3 0.1 compare_convert_fusion
  27.4 0.1 copy.66
  27.5 0.1 multiply_reduce_fusion
  27.6 0.7 reduce.18
  28.3 0.6 reshape.384
  28.9 2.2 %reshape.356 = bf16[8,224,2,128]{3,2,1,0:T(2,128)(2,1)S(1)} reshape(bf16[1,8,224,256]{3,2,1,0:T(8,128)(2,1)} %param.20) | data formatting | bytes 1835008 | tf_op jit(solution)/shard_map/reshape.7
  31.1 0.7 reduce.17
  31.7 0.6 reshape.380
  32.3 4.2 %all-to-all-start.1 = ((bf16[4,2,256]{2,1,0:T(2,128)(2,1)}), bf16[4,2,256]{2,1,0:T(2,128)(2,1)S(1)}, u32[]{:S(2)}, u32[]{:S(2)}) async-start(bf16[4,2,256]{2,1,0:T(2,128)(2,1)} %reshape.384), calls=%async_computation.1 | async-start | bytes 8192 | tf_op jit(solution)/shard_map/all_to_all | solution.py:123
  36.5 4.6 %all-to-all-done.1 = bf16[4,2,256]{2,1,0:T(2,128)(2,1)S(1)} async-done(((bf16[4,2,256]{2,1,0:T(2,128)(2,1)}), bf16[4,2,256]{2,1,0:T(2,128)(2,1)S(1)}, u32[]{:S(2)}, u32[]{:S(2)}) %all-to-all-start.1) | async-done | bytes 4128 | tf_op jit(solution)/shard_map/all_to_all | solution.py:123
  41.2 3.2 %all-to-all-start.2 = ((bf16[4,2,256]{2,1,0:T(2,128)(2,1)}), bf16[4,2,256]{2,1,0:T(2,128)(2,1)S(1)}, u32[]{:S(2)}, u32[]{:S(2)}) async-start(bf16[4,2,256]{2,1,0:T(2,128)(2,1)} %reshape.380), calls=%async_computation.2 | async-start | bytes 8192 | tf_op jit(solution)/shard_map/all_to_all | solution.py:124
  44.4 0.0 reduce-scatter.2.cloned.1.call-start
  44.6 0.1 reduce_sum.83
  44.6 0.1 reduce_sum.82
  44.8 0.2 fusion.45
  44.9 0.1 copy.79
  45.0 0.6 fusion.23
  45.6 0.1 fusion.41
  45.7 0.2 fusion.40
  45.9 0.1 divide_bitcast_fusion
  46.0 0.1 fusion.49
  46.1 3.0 %all-to-all-done.2 = bf16[4,2,256]{2,1,0:T(2,128)(2,1)S(1)} async-done(((bf16[4,2,256]{2,1,0:T(2,128)(2,1)}), bf16[4,2,256]{2,1,0:T(2,128)(2,1)S(1)}, u32[]{:S(2)}, u32[]{:S(2)}) %all-to-all-start.2) | async-done | bytes 4128 | tf_op jit(solution)/shard_map/all_to_all | solution.py:124
  49.1 1.4 %fusion.21 = f32[8,1,256]{2,1,0:T(1,128)S(1)} fusion(bf16[1,8,224,256]{3,2,1,0:T(8,128)(2,1)} %param.21, bf16[8,224,1]{1,0,2:T(8,128)(2,1)S(1)} %fusion.49), kind=kOutput, calls=%fused_computation.21 | convolution fusion | flops 917504 | bytes 929280 | tf_op jit(solution)/shard_map/sjgl,sjlv->sjgv/dot_general | solution.py:80
  50.5 0.2 multiply_reduce_fusion.1
  50.8 0.1 multiply_convert_fusion.1
  50.8 7.2 %all-gather = bf16[4,1,2048]{2,1,0:T(2,128)(2,1)S(1)} all-gather(bf16[1,1,2048]{2,1,0:T(2,128)(2,1)S(1)} %reshape.365), channel_id=1, replica_groups=mesh['ep'=8,'tp'=4] {'tp'}, dimensions={0}, use_global_device_ids=true | all-gather | bytes 20480 | tf_op jit(solution)/shard_map/all_gather | solution.py:139
  58.1 2.0 %fusion.15 = bf16[4,512]{1,0:T(4,128)(2,1)S(1)} fusion(bf16[2048,512]{1,0:T(8,128)(2,1)} %param.32, bf16[4,1,2048]{2,1,0:T(2,128)(2,1)S(1)} %all-gather, bf16[4,512]{1,0:T(4,128)(2,1)S(1)} %copy-done.4), kind=kOutput, calls=%fused_computation.12 | convolution fusion | flops 8394752 | bytes 2121728 | tf_op jit(solution)/shard_map/dot_general | solution.py:138
  60.1 8.1 %all_gather.11 = bf16[4,2048]{1,0:T(4,128)(2,1)S(1)} all-gather(bf16[4,512]{1,0:T(4,128)(2,1)S(1)} %fusion.15), channel_id=1, replica_groups=mesh['ep'=8,'tp'=4] {'tp'}, dimensions={1}, use_global_device_ids=true | all-gather | bytes 20480 | tf_op jit(solution)/shard_map/all_gather | solution.py:142
  68.2 0.1 fusion.29
  68.3 0.2 convolution_convert_fusion
  68.6 0.1 copy.68
  68.7 11.4 %all_to_all.49 = bf16[8,4,2048]{2,1,0:T(4,128)(2,1)S(1)} all-to-all(bf16[8,4,2048]{2,1,0:T(4,128)(2,1)S(1)} %copy.68), channel_id=1, replica_groups=mesh['ep'=8,'tp'=4] {'ep'}, dimensions={0} | all-to-all | bytes 262144 | tf_op jit(solution)/shard_map/all_to_all | solution.py:149
  80.2 3.2 %fusion.4 = f32[32,1024]{1,0:T(8,128)S(1)} fusion(bf16[32,2048]{1,0:T(8,128)(2,1)S(1)} %reshape.359, bf16[1,2048,1024]{2,1,0:T(8,128)(2,1)} %param.35), kind=kOutput, calls=%fused_computation.4 | convolution fusion | flops 134217728 | bytes 4456448 | tf_op jit(solution)/shard_map/dot_general | solution.py:151
  83.3 0.3 copy-done.1
  83.6 0.8 fusion.12
  84.5 3.6 %fusion.6 = bf16[8,4,2048]{2,0,1:T(8,128)(2,1)} fusion(bf16[1,1024,2048]{2,1,0:T(8,128)(2,1)} %param.37, bf16[8,4,1024]{2,1,0:T(4,128)(2,1)S(1)} %dot_general.48), kind=kOutput, calls=%fused_computation.6 | convolution fusion | flops 134283264 | bytes 4390912 | tf_op jit(solution)/shard_map/dot_general | solution.py:154
  88.1 0.0 reduce-scatter.2.cloned.1.call-update
  88.1 0.1 copy.82
  88.2 0.1 mul.249
  88.3 22.2 %reduce-scatter.2.cloned.1.call-done = bf16[8,4,512]{2,0,1:T(8,128)(2,1)} async-done(((bf16[8,4,2048]{2,0,1:T(8,128)(2,1)}), bf16[8,4,512]{2,0,1:T(8,128)(2,1)}) %reduce-scatter.2.cloned.1.call-update) | async-done | bytes 32784 | tf_op jit(solution)/shard_map/reduce_scatter | solution.py:157
  110.5 1.4 %copy.70 = bf16[8,4,512]{2,1,0:T(4,128)(2,1)} copy(bf16[8,4,512]{2,0,1:T(8,128)(2,1)} %reduce-scatter.2.cloned.1.call-done) | data formatting | bytes 65536 | tf_op jit(solution)/shard_map/reduce_scatter | solution.py:157
  111.9 4.6 %all-to-all-start.4 = ((bf16[8,4,512]{2,1,0:T(4,128)(2,1)}), bf16[8,4,512]{2,1,0:T(4,128)(2,1)S(1)}, u32[]{:S(2)}, u32[]{:S(2)}) async-start(bf16[8,4,512]{2,1,0:T(4,128)(2,1)} %copy.70), calls=%async_computation.5 | async-start | bytes 65536 | tf_op jit(solution)/shard_map/all_to_all | solution.py:160
  116.5 0.6 multiply_convert_fusion
  117.1 0.6 reshape.360
  117.7 4.5 %all-to-all-done.4 = bf16[8,4,512]{2,1,0:T(4,128)(2,1)S(1)} async-done(((bf16[8,4,512]{2,1,0:T(4,128)(2,1)}), bf16[8,4,512]{2,1,0:T(4,128)(2,1)S(1)}, u32[]{:S(2)}, u32[]{:S(2)}) %all-to-all-start.4) | async-done | bytes 32800 | tf_op jit(solution)/shard_map/all_to_all | solution.py:160
  122.2 0.8 fusion.17
  (46 shorter events, 0.4 us)
Async XLA Ops:
  7.2 10.1 %copy-start = (bf16[2048,512]{1,0:T(8,128)(2,1)S(1)}, bf16[2048,512]{1,0:T(8,128)(2,1)}, u32[]{:S(2)}) copy-start(bf16[2048,512]{1,0:T(8,128)(2,1)} %param.29) | copy-start | bytes 6291460
  7.2 16.5 %copy-start.3 = (f32[2048]{0:T(1024)S(1)}, f32[2048]{0:T(1024)}, u32[]{:S(2)}) copy-start(f32[2048]{0:T(1024)} %param.24) | copy-start | bytes 24580
  7.2 16.2 %copy-start.7 = (s32[4,2]{0,1:T(2,128)S(1)}, s32[4,2]{0,1:T(2,128)}, u32[]{:S(2)}) copy-start(s32[4,2]{0,1:T(2,128)} %param.33) | copy-start | bytes 100
  20.2 12.2 %all-to-all-start = ((bf16[4,2,256]{2,1,0:T(2,128)(2,1)}), bf16[4,2,256]{2,1,0:T(2,128)(2,1)S(1)}, u32[]{:S(2)}, u32[]{:S(2)}) async-start(bf16[4,2,256]{2,1,0:T(2,128)(2,1)} %reshape.382), calls=%async_computation | async-start | bytes 8192 | tf_op jit(solution)/shard_map/all_to_all | solution.py:122
  23.6 2.9 %copy-start.2 = (bf16[2048,512]{1,0:T(8,128)(2,1)S(1)}, bf16[2048,512]{1,0:T(8,128)(2,1)}, u32[]{:S(2)}) copy-start(bf16[2048,512]{1,0:T(8,128)(2,1)} %param.31) | copy-start | bytes 6291460
  23.7 3.7 %copy-start.8 = (f32[4,2]{0,1:T(2,128)S(1)}, f32[4,2]{0,1:T(2,128)}, u32[]{:S(2)}) copy-start(f32[4,2]{0,1:T(2,128)} %param.34) | copy-start | bytes 100
  26.5 18.2 %copy-start.10 = (f32[128]{0:T(128)S(1)}, f32[128]{0:T(128)}, u32[]{:S(2)}) copy-start(f32[128]{0:T(128)} %param.25) | copy-start | bytes 1540
  26.5 18.2 %copy-start.11 = (f32[128]{0:T(128)S(1)}, f32[128]{0:T(128)}, u32[]{:S(2)}) copy-start(f32[128]{0:T(128)} %param.26) | copy-start | bytes 1540
  27.0 19.0 %copy-start.6 = (f32[8]{0:T(128)S(1)}, f32[8]{0:T(128)}, u32[]{:S(2)}) copy-start(f32[8]{0:T(128)} %param.23) | copy-start | bytes 100
  27.0 23.8 %copy-start.9 = (f32[256]{0:T(256)S(1)}, f32[256]{0:T(256)}, u32[]{:S(2)}) copy-start(f32[256]{0:T(256)} %param.27) | copy-start | bytes 3076
  28.9 29.2 %copy-start.4 = (bf16[4,512]{1,0:T(4,128)(2,1)S(1)}, bf16[4,512]{1,0:T(4,128)(2,1)}, u32[]{:S(2)}) copy-start(bf16[4,512]{1,0:T(4,128)(2,1)} %param.19) | copy-start | bytes 12292
  32.3 8.8 %all-to-all-start.1 = ((bf16[4,2,256]{2,1,0:T(2,128)(2,1)}), bf16[4,2,256]{2,1,0:T(2,128)(2,1)S(1)}, u32[]{:S(2)}, u32[]{:S(2)}) async-start(bf16[4,2,256]{2,1,0:T(2,128)(2,1)} %reshape.384), calls=%async_computation.1 | async-start | bytes 8192 | tf_op jit(solution)/shard_map/all_to_all | solution.py:123
  41.2 7.9 %all-to-all-start.2 = ((bf16[4,2,256]{2,1,0:T(2,128)(2,1)}), bf16[4,2,256]{2,1,0:T(2,128)(2,1)S(1)}, u32[]{:S(2)}, u32[]{:S(2)}) async-start(bf16[4,2,256]{2,1,0:T(2,128)(2,1)} %reshape.380), calls=%async_computation.2 | async-start | bytes 8192 | tf_op jit(solution)/shard_map/all_to_all | solution.py:124
  44.4 66.1 %reduce-scatter.2.cloned.1.call-start = ((), (), s32[]{:S(2)}) async-start(), calls=%async_computation.6 | async-start | bytes 163840 | tf_op jit(solution)/shard_map/reduce_scatter | solution.py:157
  45.0 23.3 %copy-start.5 = (f32[2048]{0:T(1024)S(1)}, f32[2048]{0:T(1024)}, u32[]{:S(2)}) copy-start(f32[2048]{0:T(1024)} %param.28) | copy-start | bytes 24580
  80.2 3.5 %copy-start.1 = (bf16[1,2048,1024]{2,1,0:T(8,128)(2,1)S(1)}, bf16[1,2048,1024]{2,1,0:T(8,128)(2,1)}, u32[]{:S(2)}) copy-start(bf16[1,2048,1024]{2,1,0:T(8,128)(2,1)} %param.36) | copy-start | bytes 12582916
  111.9 10.3 %all-to-all-start.4 = ((bf16[8,4,512]{2,1,0:T(4,128)(2,1)}), bf16[8,4,512]{2,1,0:T(4,128)(2,1)S(1)}, u32[]{:S(2)}, u32[]{:S(2)}) async-start(bf16[8,4,512]{2,1,0:T(4,128)(2,1)} %copy.70), calls=%async_computation.5 | async-start | bytes 65536 | tf_op jit(solution)/shard_map/all_to_all | solution.py:160
Sparse Core Ops, SparseCore 0:
  88.2 22.2 reduce-scatter.1
where the time goes:
time: 131 us; the launch traced here: 130 us
  blocking collectives  36.7 us (28%)
  waiting for transfers between devices  34.4 us (26%)
  matrix products  16.3 us (12%)
  starting transfers between devices  15.3 us (12%)
  between operations  15 us (11%)
  local copies, waits for them, and re-layouts  7.69 us (6%)
  other arithmetic  4.59 us (4%)
    reduce_scatter x1, waiting for transfers between devices, local(): lax.psum_scatter(partial_value.astype(jnp.bfloat16), 'tp', scatter_dimens...  22.2 us
    all_to_all x1, blocking collectives, local(): slots = lax.all_to_all(send, 'ep', split_axis=0, concat_axis=0, tiled=True)  11.4 us
    all_gather x1, blocking collectives, local(): gathered = lax.all_gather(resid, 'tp', axis=1, tiled=True)  9.93 us
    all_gather x1, blocking collectives, local(): updated_rows = lax.all_gather(updated, 'tp', axis=1, tiled=True)  8.12 us
    all_gather x1, blocking collectives, local(): lax.all_gather(mixed, 'tp', axis=0, tiled=True)  7.25 us
    all_to_all x1, waiting for transfers between devices, local(): lax.all_to_all(key_part, 'tp', split_axis=0, concat_axis=1, tiled=True)  4.63 us
    all_to_all x1, starting transfers between devices, local(): lax.all_to_all(summed.astype(jnp.bfloat16), 'ep', split_axis=0, concat_ax...  4.6 us
    all_to_all x1, waiting for transfers between devices, local(): lax.all_to_all(summed.astype(jnp.bfloat16), 'ep', split_axis=0, concat_ax...  4.51 us
  transfers between devices with their start and end apart: 5, of which 4 were waited for; matrix products, arithmetic and copies ran while one was open for 9% of the time, Pallas kernels for 0%

commit v1 on v0

--- a/solution.py
+++ b/solution.py
@@ -139,7 +139,17 @@
         lax.all_gather(mixed, "tp", axis=0, tiled=True), w_out, preferred_element_type=jnp.float32
     )
     updated = (resid.astype(jnp.float32) + attn_proj).astype(jnp.bfloat16)
-    updated_rows = lax.all_gather(updated, "tp", axis=1, tiled=True)
+    num_devices = lax.axis_size("tp")
+    val2 = [(p - 1, p) for p in range(1, num_devices)] + [(num_devices - 1, 0)]
+    ready = updated
+    heap = [ready]
+    pp = 0
+    while pp < num_devices - 1:
+        ready = lax.ppermute(ready, "tp", val2)
+        heap += [ready]
+        pp = pp + 1
+    a_now = jnp.concatenate([*reversed(heap)], axis=1)
+    updated_rows = jnp.roll(a_now, (lax.axis_index("tp") + 1) * ready.shape[1], axis=1)
     hidden = scaled_rows(updated_rows, ffn_gain).astype(jnp.bfloat16)
     experts = w_gate.shape[0] * lax.axis_size("ep")
     dispatch, combine = route_tables(routes, route_weights, experts, CAP)

time: 131 us -> 136 us (1.038)
  waiting for transfers between devices: 34.4 us -> 45.4 us
  blocking collectives: 36.7 us -> 28.6 us
  starting transfers between devices: 15.3 us -> 17.3 us
    ppermute x0 -> x3, waiting for transfers between devices: none -> 11 us  [local(): ready = lax.ppermute(ready, 'tp', val2)]
    all_gather x1 -> x0, blocking collectives: 8.12 us -> none  [local(): updated_rows = lax.all_gather(updated, 'tp', axis=1, tiled=True)]
    ppermute x0 -> x3, starting transfers between devices: none -> 2.02 us  [local(): ready = lax.ppermute(ready, 'tp', val2)]
  transfers between devices with their start and end apart: 5 -> 8, of which waited for: 4 -> 7; matrix products, arithmetic and copies ran while one was open for 9% -> 8% of each run, Pallas kernels for 0% -> 0%
where the time goes in v1:
time: 136 us; the launch traced here: 135 us
  waiting for transfers between devices  45.4 us (33%)
  blocking collectives  28.6 us (21%)
  starting transfers between devices  17.3 us (13%)
  matrix products  16.3 us (12%)
  between operations  15 us (11%)
  local copies, waits for them, and re-layouts  7.78 us (6%)
  other arithmetic  4.58 us (3%)
    reduce_scatter x1, waiting for transfers between devices, local(): lax.psum_scatter(partial_value.astype(jnp.bfloat16), 'tp', scatter_dimens...  22.2 us
    all_to_all x1, blocking collectives, local(): slots = lax.all_to_all(send, 'ep', split_axis=0, concat_axis=0, tiled=True)  11.4 us
    ppermute x3, waiting for transfers between devices, local(): ready = lax.ppermute(ready, 'tp', val2)  11 us
    all_gather x1, blocking collectives, local(): gathered = lax.all_gather(resid, 'tp', axis=1, tiled=True)  9.93 us
    all_gather x1, blocking collectives, local(): lax.all_gather(mixed, 'tp', axis=0, tiled=True)  7.25 us
    all_to_all x1, waiting for transfers between devices, local(): lax.all_to_all(key_part, 'tp', split_axis=0, concat_axis=1, tiled=True)  4.63 us
    all_to_all x1, starting transfers between devices, local(): lax.all_to_all(summed.astype(jnp.bfloat16), 'ep', split_axis=0, concat_ax...  4.6 us
    all_to_all x1, waiting for transfers between devices, local(): lax.all_to_all(summed.astype(jnp.bfloat16), 'ep', split_axis=0, concat_ax...  4.51 us
  transfers between devices with their start and end apart: 8, of which 7 were waited for; matrix products, arithmetic and copies ran while one was open for 8% of the time, Pallas kernels for 0%

profile of v1, /device:TPU:0, one launch (start us, length us, event | category | flops | bytes accessed | tf_op | source)
XLA Modules:
  0.0 134.9 jit_solution(3933955574215006943)
XLA Ops:
  7.2 9.9 %all_gather.6 = bf16[4,2048]{1,0:T(4,128)(2,1)S(1)} all-gather(bf16[4,512]{1,0:T(4,128)(2,1)} %param.19), channel_id=1, replica_groups=mesh['ep'=8,'tp'=4] {'tp'}, dimensions={1}, use_global_device_ids=true | all-gather | bytes 20480 | tf_op jit(solution)/shard_map/all_gather | solution.py:116
  17.1 0.1 fusion.26
  17.3 1.1 fusion.18
  18.4 0.5 broadcast.215
  18.9 0.7 reduce.19
  19.6 0.6 reshape.382
  20.2 3.2 %all-to-all-start = ((bf16[4,2,256]{2,1,0:T(2,128)(2,1)}), bf16[4,2,256]{2,1,0:T(2,128)(2,1)S(1)}, u32[]{:S(2)}, u32[]{:S(2)}) async-start(bf16[4,2,256]{2,1,0:T(2,128)(2,1)} %reshape.382), calls=%async_computation | async-start | bytes 8192 | tf_op jit(solution)/shard_map/all_to_all | solution.py:122
  23.4 0.1 copy.64
  23.5 0.1 eq.50
  23.6 0.1 fusion.49
  23.7 2.1 %fusion.19 = bf16[4,1,512]{2,0,1:T(4,128)(2,1)S(1)} fusion(bf16[2048,512]{1,0:T(8,128)(2,1)} %param.30, bf16[4,2048]{1,0:T(4,128)(2,1)S(1)} %all_gather.6, f32[2048]{0:T(1024)S(1)} %copy-done.3, f32[4]{0:T(128)S(1)} %add_rsqrt_fusion.4), kind=kOutput, calls=%fused_computation.19 | convolution fusion | flops 8423424 | bytes 2125840 | tf_op jit(solution)/shard_map/dot_general | solution.py:119
  26.6 0.4 fusion.20
  27.0 0.1 fusion.52
  27.1 0.7 reduce.18
  27.7 0.6 reshape.384
  28.3 2.2 %reshape.356 = bf16[8,224,2,128]{3,2,1,0:T(2,128)(2,1)S(1)} reshape(bf16[1,8,224,256]{3,2,1,0:T(8,128)(2,1)} %param.20) | data formatting | bytes 1835008 | tf_op jit(solution)/shard_map/reshape.7
  30.5 0.7 reduce.17
  31.2 0.6 reshape.380
  31.8 4.2 %all-to-all-start.1 = ((bf16[4,2,256]{2,1,0:T(2,128)(2,1)}), bf16[4,2,256]{2,1,0:T(2,128)(2,1)S(1)}, u32[]{:S(2)}, u32[]{:S(2)}) async-start(bf16[4,2,256]{2,1,0:T(2,128)(2,1)} %reshape.384), calls=%async_computation.1 | async-start | bytes 8192 | tf_op jit(solution)/shard_map/all_to_all | solution.py:123
  36.0 4.6 %all-to-all-done.1 = bf16[4,2,256]{2,1,0:T(2,128)(2,1)S(1)} async-done(((bf16[4,2,256]{2,1,0:T(2,128)(2,1)}), bf16[4,2,256]{2,1,0:T(2,128)(2,1)S(1)}, u32[]{:S(2)}, u32[]{:S(2)}) %all-to-all-start.1) | async-done | bytes 4128 | tf_op jit(solution)/shard_map/all_to_all | solution.py:123
  40.6 3.2 %all-to-all-start.2 = ((bf16[4,2,256]{2,1,0:T(2,128)(2,1)}), bf16[4,2,256]{2,1,0:T(2,128)(2,1)S(1)}, u32[]{:S(2)}, u32[]{:S(2)}) async-start(bf16[4,2,256]{2,1,0:T(2,128)(2,1)} %reshape.380), calls=%async_computation.2 | async-start | bytes 8192 | tf_op jit(solution)/shard_map/all_to_all | solution.py:124
  43.9 0.0 reduce-scatter.2.cloned.1.call-start
  44.0 0.1 reduce_sum.83
  44.1 0.1 reduce_sum.82
  44.2 0.2 fusion.46
  44.4 0.1 copy.79
  44.5 0.6 fusion.23
  45.0 0.1 fusion.42
  45.1 0.2 fusion.40
  45.3 0.1 divide_bitcast_fusion
  45.4 0.1 fusion.50
  45.5 3.0 %all-to-all-done.2 = bf16[4,2,256]{2,1,0:T(2,128)(2,1)S(1)} async-done(((bf16[4,2,256]{2,1,0:T(2,128)(2,1)}), bf16[4,2,256]{2,1,0:T(2,128)(2,1)S(1)}, u32[]{:S(2)}, u32[]{:S(2)}) %all-to-all-start.2) | async-done | bytes 4128 | tf_op jit(solution)/shard_map/all_to_all | solution.py:124
  48.6 1.4 %fusion.21 = f32[8,1,256]{2,1,0:T(1,128)S(1)} fusion(bf16[1,8,224,256]{3,2,1,0:T(8,128)(2,1)} %param.21, bf16[8,224,1]{1,0,2:T(8,128)(2,1)S(1)} %fusion.50), kind=kOutput, calls=%fused_computation.21 | convolution fusion | flops 917504 | bytes 929280 | tf_op jit(solution)/shard_map/sjgl,sjlv->sjgv/dot_general | solution.py:80
  50.0 0.2 multiply_reduce_fusion.1
  50.2 0.1 multiply_convert_fusion.1
  50.3 7.2 %all-gather = bf16[4,1,2048]{2,1,0:T(2,128)(2,1)S(1)} all-gather(bf16[1,1,2048]{2,1,0:T(2,128)(2,1)S(1)} %reshape.365), channel_id=1, replica_groups=mesh['ep'=8,'tp'=4] {'tp'}, dimensions={0}, use_global_device_ids=true | all-gather | bytes 20480 | tf_op jit(solution)/shard_map/all_gather | solution.py:139
  57.6 2.0 %fusion.15 = bf16[4,512]{1,0:T(4,128)(2,1)S(1)} fusion(bf16[2048,512]{1,0:T(8,128)(2,1)} %param.32, bf16[4,1,2048]{2,1,0:T(2,128)(2,1)S(1)} %all-gather, bf16[4,512]{1,0:T(4,128)(2,1)S(1)} %copy-done.4), kind=kOutput, calls=%fused_computation.12 | convolution fusion | flops 8394752 | bytes 2121728 | tf_op jit(solution)/shard_map/dot_general | solution.py:138
  59.5 1.5 %collective-permute-start = (bf16[4,512]{1,0:T(4,128)(2,1)S(1)}, bf16[4,512]{1,0:T(4,128)(2,1)S(1)}, u32[]{:S(2)}, u32[]{:S(2)}) collective-permute-start(bf16[4,512]{1,0:T(4,128)(2,1)S(1)} %fusion.15), channel_id=1, source_target_pairs={{0,1},{1,2},{2,3},{3,0},{4,5},{5,6},{6,7},{7,4},{8,9},{9,10},{10,1... | collective-permute-start | bytes 12296 | tf_op jit(solution)/shard_map/ppermute | solution.py:148
  61.0 0.2 select_reduce_fusion
  61.2 0.1 eq.54
  61.3 2.8 %collective-permute-done = bf16[4,512]{1,0:T(4,128)(2,1)S(1)} collective-permute-done((bf16[4,512]{1,0:T(4,128)(2,1)S(1)}, bf16[4,512]{1,0:T(4,128)(2,1)S(1)}, u32[]{:S(2)}, u32[]{:S(2)}) %collective-permute-start) | collective-permute-done | bytes 4128 | tf_op jit(solution)/shard_map/ppermute | solution.py:148
  64.1 0.6 collective-permute-start.1
  64.6 0.1 compare_convert_fusion
  64.7 0.1 copy.66
  64.8 3.8 %collective-permute-done.1 = bf16[4,512]{1,0:T(4,128)(2,1)S(1)} collective-permute-done((bf16[4,512]{1,0:T(4,128)(2,1)S(1)}, bf16[4,512]{1,0:T(4,128)(2,1)S(1)}, u32[]{:S(2)}, u32[]{:S(2)}) %collective-permute-start.1) | collective-permute-done | bytes 4128 | tf_op jit(solution)/shard_map/ppermute | solution.py:148
  68.6 0.1 multiply_reduce_fusion
  68.7 4.4 %collective-permute-done.2 = bf16[4,512]{1,0:T(4,128)(2,1)S(1)} collective-permute-done((bf16[4,512]{1,0:T(4,128)(2,1)S(1)}, bf16[4,512]{1,0:T(4,128)(2,1)S(1)}, u32[]{:S(2)}, u32[]{:S(2)}) %collective-permute-start.2) | collective-permute-done | bytes 4128 | tf_op jit(solution)/shard_map/ppermute | solution.py:148
  73.2 0.1 fusion.29
  73.3 0.2 convolution_convert_fusion
  73.6 0.1 copy.68
  73.7 11.4 %all_to_all.49 = bf16[8,4,2048]{2,1,0:T(4,128)(2,1)S(1)} all-to-all(bf16[8,4,2048]{2,1,0:T(4,128)(2,1)S(1)} %copy.68), channel_id=1, replica_groups=mesh['ep'=8,'tp'=4] {'ep'}, dimensions={0} | all-to-all | bytes 262144 | tf_op jit(solution)/shard_map/all_to_all | solution.py:159
  85.2 3.2 %fusion.4 = f32[32,1024]{1,0:T(8,128)S(1)} fusion(bf16[32,2048]{1,0:T(8,128)(2,1)S(1)} %reshape.359, bf16[1,2048,1024]{2,1,0:T(8,128)(2,1)} %param.35), kind=kOutput, calls=%fused_computation.4 | convolution fusion | flops 134217728 | bytes 4456448 | tf_op jit(solution)/shard_map/dot_general | solution.py:161
  88.3 0.3 copy-done.1
  88.6 0.8 fusion.12
  89.5 3.6 %fusion.6 = bf16[8,4,2048]{2,0,1:T(8,128)(2,1)} fusion(bf16[1,1024,2048]{2,1,0:T(8,128)(2,1)} %param.37, bf16[8,4,1024]{2,1,0:T(4,128)(2,1)S(1)} %dot_general.48), kind=kOutput, calls=%fused_computation.6 | convolution fusion | flops 134283264 | bytes 4390912 | tf_op jit(solution)/shard_map/dot_general | solution.py:164
  93.1 0.1 copy.82
  93.2 0.1 mul.252
  93.3 22.2 %reduce-scatter.2.cloned.1.call-done = bf16[8,4,512]{2,0,1:T(8,128)(2,1)} async-done(((bf16[8,4,2048]{2,0,1:T(8,128)(2,1)}), bf16[8,4,512]{2,0,1:T(8,128)(2,1)}) %reduce-scatter.2.cloned.1.call-update) | async-done | bytes 32784 | tf_op jit(solution)/shard_map/reduce_scatter | solution.py:167
  115.5 1.4 %copy.70 = bf16[8,4,512]{2,1,0:T(4,128)(2,1)} copy(bf16[8,4,512]{2,0,1:T(8,128)(2,1)} %reduce-scatter.2.cloned.1.call-done) | data formatting | bytes 65536 | tf_op jit(solution)/shard_map/reduce_scatter | solution.py:167
  116.9 4.6 %all-to-all-start.4 = ((bf16[8,4,512]{2,1,0:T(4,128)(2,1)}), bf16[8,4,512]{2,1,0:T(4,128)(2,1)S(1)}, u32[]{:S(2)}, u32[]{:S(2)}) async-start(bf16[8,4,512]{2,1,0:T(4,128)(2,1)} %copy.70), calls=%async_computation.5 | async-start | bytes 65536 | tf_op jit(solution)/shard_map/all_to_all | solution.py:170
  121.5 0.6 multiply_convert_fusion
  122.1 0.6 reshape.360
  122.7 4.5 %all-to-all-done.4 = bf16[8,4,512]{2,1,0:T(4,128)(2,1)S(1)} async-done(((bf16[8,4,512]{2,1,0:T(4,128)(2,1)}), bf16[8,4,512]{2,1,0:T(4,128)(2,1)S(1)}, u32[]{:S(2)}, u32[]{:S(2)}) %all-to-all-start.4) | async-done | bytes 32800 | tf_op jit(solution)/shard_map/all_to_all | solution.py:170
  127.2 0.8 fusion.17
  (59 shorter events, 0.5 us)
Async XLA Ops:
  7.2 10.1 %copy-start = (bf16[2048,512]{1,0:T(8,128)(2,1)S(1)}, bf16[2048,512]{1,0:T(8,128)(2,1)}, u32[]{:S(2)}) copy-start(bf16[2048,512]{1,0:T(8,128)(2,1)} %param.29) | copy-start | bytes 6291460
  7.2 16.5 %copy-start.3 = (f32[2048]{0:T(1024)S(1)}, f32[2048]{0:T(1024)}, u32[]{:S(2)}) copy-start(f32[2048]{0:T(1024)} %param.24) | copy-start | bytes 24580
  7.2 16.2 %copy-start.7 = (s32[4,2]{0,1:T(2,128)S(1)}, s32[4,2]{0,1:T(2,128)}, u32[]{:S(2)}) copy-start(s32[4,2]{0,1:T(2,128)} %param.33) | copy-start | bytes 100
  20.2 11.6 %all-to-all-start = ((bf16[4,2,256]{2,1,0:T(2,128)(2,1)}), bf16[4,2,256]{2,1,0:T(2,128)(2,1)S(1)}, u32[]{:S(2)}, u32[]{:S(2)}) async-start(bf16[4,2,256]{2,1,0:T(2,128)(2,1)} %reshape.382), calls=%async_computation | async-start | bytes 8192 | tf_op jit(solution)/shard_map/all_to_all | solution.py:122
  23.6 2.9 %copy-start.2 = (bf16[2048,512]{1,0:T(8,128)(2,1)S(1)}, bf16[2048,512]{1,0:T(8,128)(2,1)}, u32[]{:S(2)}) copy-start(bf16[2048,512]{1,0:T(8,128)(2,1)} %param.31) | copy-start | bytes 6291460
  25.8 18.4 %copy-start.10 = (f32[128]{0:T(128)S(1)}, f32[128]{0:T(128)}, u32[]{:S(2)}) copy-start(f32[128]{0:T(128)} %param.25) | copy-start | bytes 1540
  25.8 18.4 %copy-start.11 = (f32[128]{0:T(128)S(1)}, f32[128]{0:T(128)}, u32[]{:S(2)}) copy-start(f32[128]{0:T(128)} %param.26) | copy-start | bytes 1540
  26.5 18.9 %copy-start.6 = (f32[8]{0:T(128)S(1)}, f32[8]{0:T(128)}, u32[]{:S(2)}) copy-start(f32[8]{0:T(128)} %param.23) | copy-start | bytes 100
  27.0 23.2 %copy-start.8 = (f32[256]{0:T(256)S(1)}, f32[256]{0:T(256)}, u32[]{:S(2)}) copy-start(f32[256]{0:T(256)} %param.27) | copy-start | bytes 3076
  28.3 29.2 %copy-start.4 = (bf16[4,512]{1,0:T(4,128)(2,1)S(1)}, bf16[4,512]{1,0:T(4,128)(2,1)}, u32[]{:S(2)}) copy-start(bf16[4,512]{1,0:T(4,128)(2,1)} %param.19) | copy-start | bytes 12292
  31.8 8.8 %all-to-all-start.1 = ((bf16[4,2,256]{2,1,0:T(2,128)(2,1)}), bf16[4,2,256]{2,1,0:T(2,128)(2,1)S(1)}, u32[]{:S(2)}, u32[]{:S(2)}) async-start(bf16[4,2,256]{2,1,0:T(2,128)(2,1)} %reshape.384), calls=%async_computation.1 | async-start | bytes 8192 | tf_op jit(solution)/shard_map/all_to_all | solution.py:123
  40.6 7.9 %all-to-all-start.2 = ((bf16[4,2,256]{2,1,0:T(2,128)(2,1)}), bf16[4,2,256]{2,1,0:T(2,128)(2,1)S(1)}, u32[]{:S(2)}, u32[]{:S(2)}) async-start(bf16[4,2,256]{2,1,0:T(2,128)(2,1)} %reshape.380), calls=%async_computation.2 | async-start | bytes 8192 | tf_op jit(solution)/shard_map/all_to_all | solution.py:124
  43.9 71.6 %reduce-scatter.2.cloned.1.call-start = ((), (), s32[]{:S(2)}) async-start(), calls=%async_computation.6 | async-start | bytes 163840 | tf_op jit(solution)/shard_map/reduce_scatter | solution.py:167
  44.5 20.2 %copy-start.9 = (f32[4,2]{0,1:T(2,128)S(1)}, f32[4,2]{0,1:T(2,128)}, u32[]{:S(2)}) copy-start(f32[4,2]{0,1:T(2,128)} %param.34) | copy-start | bytes 100
  44.5 28.8 %copy-start.5 = (f32[2048]{0:T(1024)S(1)}, f32[2048]{0:T(1024)}, u32[]{:S(2)}) copy-start(f32[2048]{0:T(1024)} %param.28) | copy-start | bytes 24580
  59.5 4.5 %collective-permute-start = (bf16[4,512]{1,0:T(4,128)(2,1)S(1)}, bf16[4,512]{1,0:T(4,128)(2,1)S(1)}, u32[]{:S(2)}, u32[]{:S(2)}) collective-permute-start(bf16[4,512]{1,0:T(4,128)(2,1)S(1)} %fusion.15), channel_id=1, source_target_pairs={{0,1},{1,2},{2,3},{3,0},{4,5},{5,6},{6,7},{7,4},{8,9},{9,10},{10,1... | collective-permute-start | bytes 12296 | tf_op jit(solution)/shard_map/ppermute | solution.py:148
  64.1 4.5 %collective-permute-start.1 = (bf16[4,512]{1,0:T(4,128)(2,1)S(1)}, bf16[4,512]{1,0:T(4,128)(2,1)S(1)}, u32[]{:S(2)}, u32[]{:S(2)}) collective-permute-start(bf16[4,512]{1,0:T(4,128)(2,1)S(1)} %collective-permute-done), channel_id=1, source_target_pairs={{0,1},{1,2},{2,3},{3,0},{4,5},{5,6},{6,7},{7,4},{8,9},{9,10},{10,1... | collective-permute-start | bytes 12296 | tf_op jit(solution)/shard_map/ppermute | solution.py:148
  68.6 4.5 %collective-permute-start.2 = (bf16[4,512]{1,0:T(4,128)(2,1)S(1)}, bf16[4,512]{1,0:T(4,128)(2,1)S(1)}, u32[]{:S(2)}, u32[]{:S(2)}) collective-permute-start(bf16[4,512]{1,0:T(4,128)(2,1)S(1)} %collective-permute-done.1), channel_id=1, source_target_pairs={{0,1},{1,2},{2,3},{3,0},{4,5},{5,6},{6,7},{7,4},{8,9},{9,10},{10,1... | collective-permute-start | bytes 12296 | tf_op jit(solution)/shard_map/ppermute | solution.py:148
  85.1 3.5 %copy-start.1 = (bf16[1,2048,1024]{2,1,0:T(8,128)(2,1)S(1)}, bf16[1,2048,1024]{2,1,0:T(8,128)(2,1)}, u32[]{:S(2)}) copy-start(bf16[1,2048,1024]{2,1,0:T(8,128)(2,1)} %param.36) | copy-start | bytes 12582916
  116.9 10.3 %all-to-all-start.4 = ((bf16[8,4,512]{2,1,0:T(4,128)(2,1)}), bf16[8,4,512]{2,1,0:T(4,128)(2,1)S(1)}, u32[]{:S(2)}, u32[]{:S(2)}) async-start(bf16[8,4,512]{2,1,0:T(4,128)(2,1)} %copy.70), calls=%async_computation.5 | async-start | bytes 65536 | tf_op jit(solution)/shard_map/all_to_all | solution.py:170
Sparse Core Ops, SparseCore 0:
  93.2 22.2 reduce-scatter.1
